TPU v7x, 32 devices: a whole 2x2x4 slice. The times are simulated.
32 devices in a mesh: sp: 4 (over z), fs: 4 (over y, x), tp: 2 (over core).
Axes of the slice: x: 2, y: 2, z: 4, core: 2. Of those that a mesh axis runs over, the one named last changes fastest.
Arguments:
- tokens: bfloat16 [2048, 2048], P('sp', ('fs', 'tp')), may hold values from -6 to 6
- in_gain: float32 [2048], replicated, may hold values from 0.1 to 1.9
- conv_a_weight: bfloat16 [2048, 1024], P(None, ('fs', 'tp')), may hold values from -0.125 to 0.125
- conv_gate_weight: bfloat16 [2048, 1024], P(None, ('fs', 'tp')), may hold values from -0.125 to 0.125
- query_weight: bfloat16 [2048, 1024], P(None, ('fs', 'tp')), may hold values from -0.125 to 0.125
- key_weight: bfloat16 [2048, 1024], P(None, ('fs', 'tp')), may hold values from -0.125 to 0.125
- value_weight: bfloat16 [2048, 1024], P(None, ('fs', 'tp')), may hold values from -0.125 to 0.125
- conv_taps: bfloat16 [31, 1024], replicated, may hold values from -3 to 3
- conv_norm_gain: float32 [1024], replicated, may hold values from 0.1 to 1.9
- break_shift: bfloat16 [16, 2048], P(('fs', 'tp'), 'sp'), may hold values from -20 to 1
- conv_out_gain: float32 [1024], replicated, may hold values from 0.1 to 1.9
- attn_out_gain: float32 [1024], replicated, may hold values from 0.1 to 1.9
- out_weight: bfloat16 [2048, 2048], P(None, ('fs', 'tp')), may hold values from -0.125 to 0.125
Outputs:
- mixed: bfloat16 [2048, 2048], P('sp', ('fs', 'tp'))
All inputs are finite; a program needn't handle non-finite values.
Results may differ from a plain program's by a relative error of at most 0.0078.
Values may be sent and summed in bfloat16 or wider, within the bound.
A program may use at most 128 MiB of HBM per device.

v0:
```python
import jax
import jax.numpy as jnp
from jax import lax
from jax.sharding import PartitionSpec as P

HEAD_DIM = 64
epsilon = 1e-06


def passed_along(shard, axis, by):
    count = lax.axis_size(axis)
    pairs = [(i, i + by) for i in range(count) if 0 <= i + by < count]
    return lax.ppermute(shard, axis, pairs)


def per_device(
    tokens,
    in_gain,
    conv_a_weight,
    conv_gate_weight,
    query_weight,
    key_weight,
    value_weight,
    conv_taps,
    conv_norm_gain,
    break_shift,
    conv_out_gain,
    attn_out_gain,
    out_weight,
):
    rows_here = tokens.shape[0]
    model_width = in_gain.shape[0]
    channels = model_width // 2
    local_width = conv_a_weight.shape[1]
    heads_here = break_shift.shape[0]
    group_index = lax.axis_index(("fs", "tp"))
    shard_index = lax.axis_index("sp")
    stacked = jnp.concatenate(
        (conv_a_weight, conv_gate_weight, query_weight, key_weight, value_weight), axis=1
    )
    segment = lax.all_gather(tokens, ("fs", "tp"), axis=1, tiled=True)
    segment_wide = segment.astype(jnp.float32)
    scaled = (segment_wide * in_gain[None, :]).astype(jnp.bfloat16)
    totals = jnp.dot(scaled, stacked, preferred_element_type=jnp.float32)
    totals, squares = (totals, jnp.sum(segment_wide * segment_wide, axis=1))
    input_scale = lax.rsqrt(squares / model_width + epsilon)
    projected = (totals * input_scale[:, None]).astype(jnp.bfloat16)
    conv_a = projected[:, :local_width]
    conv_gate = projected[:, local_width : 2 * local_width]
    query = projected[:, 2 * local_width : 3 * local_width]
    key = projected[:, 3 * local_width : 4 * local_width]
    value = projected[:, 4 * local_width :]
    gated_input = conv_a.astype(jnp.float32) * jax.nn.sigmoid(conv_gate.astype(jnp.float32))
    reach_rows = conv_taps.shape[0] - 1
    earlier = passed_along(gated_input[rows_here - reach_rows :], "sp", 1)
    padded = jnp.concatenate((earlier, gated_input), axis=0)
    tap_values = lax.dynamic_slice_in_dim(
        conv_taps, group_index * local_width, local_width, 1
    ).astype(jnp.float32)
    conv_out = jnp.zeros((rows_here, local_width), jnp.float32)
    for offset in range(reach_rows + 1):
        conv_out = conv_out + tap_values[offset][None, :] * padded[offset : offset + rows_here]
    first_sum, second_sum = lax.psum(
        (jnp.sum(conv_out, axis=1), jnp.sum(conv_out * conv_out, axis=1)), ("fs", "tp")
    )
    row_mean = first_sum / channels
    row_spread = second_sum / channels - row_mean * row_mean
    centered = conv_out - row_mean[:, None]
    norm_gain = lax.dynamic_slice_in_dim(conv_norm_gain, group_index * local_width, local_width, 0)
    normed = centered * lax.rsqrt(row_spread + epsilon)[:, None] * norm_gain[None, :]
    conv_mixed = jax.nn.silu(normed).astype(jnp.bfloat16)
    queries = query.reshape(rows_here, heads_here, HEAD_DIM)
    query_pos = shard_index * rows_here + jnp.arange(rows_here, dtype=jnp.int32)
    score_scale = HEAD_DIM ** (-0.5)

    def attend(running, key_rows, value_rows, shift_rows, start_pos):
        outputs, behind = running
        piece_rows = key_rows.shape[0]
        key_heads = key_rows.reshape(piece_rows, heads_here, HEAD_DIM)
        value_heads = value_rows.reshape(piece_rows, heads_here, HEAD_DIM)
        scores = (
            jnp.einsum("qhd,khd->hqk", queries, key_heads, preferred_element_type=jnp.float32)
            * score_scale
        )
        scores = scores + shift_rows.astype(jnp.float32)[:, None, :]
        key_pos = start_pos + jnp.arange(piece_rows, dtype=jnp.int32)
        allowed = ((key_pos[None, :] < query_pos[:, None]) & (key_pos[None, :] >= 0))[None]
        log_fail = jnp.where(allowed, jax.nn.log_sigmoid(-scores), 0.0)
        later_sum = lax.cumsum(log_fail, axis=2, reverse=True) - log_fail + behind[:, :, None]
        weights = jnp.where(allowed, jnp.exp(jax.nn.log_sigmoid(scores) + later_sum), 0.0).astype(
            jnp.bfloat16
        )
        outputs = outputs + jnp.einsum(
            "hqk,khd->qhd", weights, value_heads, preferred_element_type=jnp.float32
        )
        return (outputs, behind + jnp.sum(log_fail, axis=2))

    start_state = (
        jnp.zeros((rows_here, heads_here, HEAD_DIM), jnp.float32),
        jnp.zeros((heads_here, rows_here), jnp.float32),
    )
    all_keys, all_values, all_shifts = (
        lax.all_gather(key, "sp", axis=0, tiled=True),
        lax.all_gather(value, "sp", axis=0, tiled=True),
        lax.all_gather(break_shift, "sp", axis=1, tiled=True),
    )
    sp_count = lax.axis_size("sp")
    grouped = 1
    while grouped * 2 * rows_here <= 1024 and sp_count % (grouped * 2) == 0:
        grouped = grouped * 2
    block_rows = grouped * rows_here
    last_block = (shard_index * rows_here + rows_here - 1) // block_rows

    def advance(counter, running):
        begin_row = (last_block - counter) * block_rows
        key_rows = lax.dynamic_slice_in_dim(all_keys, begin_row, block_rows, 0)
        value_rows = lax.dynamic_slice_in_dim(all_values, begin_row, block_rows, 0)
        shift_rows = lax.dynamic_slice_in_dim(all_shifts, begin_row, block_rows, 1)
        return attend(running, key_rows, value_rows, shift_rows, begin_row)

    outputs, behind = lax.fori_loop(0, last_block + 1, advance, start_state)
    attn_mixed = outputs.reshape(rows_here, heads_here * HEAD_DIM).astype(jnp.bfloat16)
    conv_piece = lax.all_gather(conv_mixed, ("fs", "tp"), axis=1, tiled=True)
    attn_piece = lax.all_gather(attn_mixed, ("fs", "tp"), axis=1, tiled=True)
    piece_width = conv_piece.shape[1]
    conv_wide = conv_piece.astype(jnp.float32)
    attn_wide = attn_piece.astype(jnp.float32)
    conv_scaled = (conv_wide * conv_out_gain[None, :]).astype(jnp.bfloat16)
    attn_scaled = (attn_wide * attn_out_gain[None, :]).astype(jnp.bfloat16)
    conv_rows = lax.slice_in_dim(out_weight, 0, piece_width, axis=0)
    attn_rows = lax.dynamic_slice_in_dim(out_weight, channels, piece_width, 0)
    conv_total = jnp.dot(conv_scaled, conv_rows, preferred_element_type=jnp.float32)
    attn_total = jnp.dot(attn_scaled, attn_rows, preferred_element_type=jnp.float32)
    conv_squares = jnp.sum(conv_wide * conv_wide, axis=1)
    attn_squares = jnp.sum(attn_wide * attn_wide, axis=1)
    conv_total, attn_total, conv_squares, attn_squares = (
        conv_total,
        attn_total,
        conv_squares,
        attn_squares,
    )
    conv_scale = lax.rsqrt(conv_squares / channels + epsilon)
    attn_scale = lax.rsqrt(attn_squares / channels + epsilon)
    mixed = conv_total * conv_scale[:, None] + attn_total * attn_scale[:, None]
    return mixed.astype(jnp.bfloat16)


def solution(mesh):
    return jax.shard_map(
        per_device,
        mesh=mesh,
        in_specs=(
            P("sp", ("fs", "tp")),
            P(),
            P(None, ("fs", "tp")),
            P(None, ("fs", "tp")),
            P(None, ("fs", "tp")),
            P(None, ("fs", "tp")),
            P(None, ("fs", "tp")),
            P(),
            P(),
            P(("fs", "tp"), "sp"),
            P(),
            P(),
            P(None, ("fs", "tp")),
        ),
        out_specs=P("sp", ("fs", "tp")),
        check_vma=False,
    )
```

profile of v0, /device:TPU:0, one launch (start us, length us, event | category | flops | bytes accessed | tf_op | source)
XLA Modules:
  0.0 200.8 jit_solution(11392080675907995282)
XLA Ops:
  6.5 0.7 all-gather.4.cloned.1.call-update
  7.3 13.8 %all_gather.22 = bf16[2,2048]{1,0:T(2,128)(2,1)S(1)} all-gather(bf16[2,512]{1,0:T(2,128)(2,1)} %param.24), channel_id=1, replica_groups=mesh['sp'=4,'fs'=4,'tp'=2] {'sp'}, dimensions={1}, use_global_device_ids=true | all-gather | bytes 10240 | tf_op jit(solution)/shard_map/all_gather | solution.py:105
  21.1 1.9 constant_dynamic-update-slice_fusion.4
  23.0 1.9 constant_dynamic-update-slice_fusion.3
  24.9 1.9 constant_dynamic-update-slice_fusion.2
  26.9 1.9 constant_dynamic-update-slice_fusion.1
  28.8 0.9 constant_dynamic-update-slice_fusion
  29.6 10.4 %all-gather.4.cloned.1.call-done = bf16[512,2048]{1,0:T(8,128)(2,1)} async-done(((bf16[512,256]{1,0:T(8,128)(2,1)}), bf16[512,2048]{1,0:T(8,128)(2,1)}) %all-gather.4.cloned.1.call-update) | async-done | bytes 2097168 | tf_op jit(solution)/shard_map/all_gather | solution.py:41
  40.1 2.1 %fusion.19 = f32[512]{0:T(512)S(1)} fusion(bf16[512,2048]{1,0:T(8,128)(2,1)} %all-gather.4.cloned.1.call-done), kind=kLoop, calls=%fused_computation.37 | loop fusion | flops 3145216 | bytes 2099200 | tf_op jit(solution)/shard_map/reduce_sum | solution.py:45
  42.2 4.2 %fusion.30 = bf16[512,640]{1,0:T(8,128)(2,1)S(1)} fusion(bf16[2048,640]{1,0:T(8,128)(2,1)} %constant_dynamic-update-slice_fusion, bf16[512,2048]{1,0:T(8,128)(2,1)} %all-gather.4.cloned.1.call-done, f32[2048]{0:T(1024)S(1)} %copy-done.4, f32[512]{0:T(512)S(1)} %add_rsqrt_fusion.3), kind=kOutput, calls=%fused_computation.78 | convolution fusion | flops 1345978368 | bytes 5384192 | tf_op jit(solution)/shard_map/dot_general | solution.py:44
  46.4 16.1 %all_gather.20 = bf16[2048,128]{1,0:T(8,128)(2,1)S(1)} all-gather(bf16[512,128]{1,0:T(8,128)(2,1)S(1)} %get-tuple-element.135), channel_id=1, replica_groups=mesh['sp'=4,'fs'=4,'tp'=2] {'sp'}, dimensions={0}, use_global_device_ids=true | all-gather | bytes 655360 | tf_op jit(solution)/shard_map/all_gather | solution.py:104
  62.5 16.0 %all_gather.21 = bf16[2048,128]{1,0:T(8,128)(2,1)S(1)} all-gather(bf16[512,128]{1,0:T(8,128)(2,1)S(1)} %get-tuple-element.134), channel_id=1, replica_groups=mesh['sp'=4,'fs'=4,'tp'=2] {'sp'}, dimensions={0}, use_global_device_ids=true | all-gather | bytes 655360 | tf_op jit(solution)/shard_map/all_gather | solution.py:103
  78.7 31.2 %while.13 = (s32[]{:T(128)}, f32[512,2,64]{0,2,1:T(8,128)S(1)}, f32[2,512]{1,0:T(2,128)S(1)}, s32[]{:T(128)}, s32[]{:T(128)}, /*index=5*/bf16[2048,128]{1,0:T(8,...) while((s32[]{:T(128)}, f32[512,2,64]{0,2,1:T(8,128)S(1)}, ...), condition=%wide.region_10.11_spmd.clone, body=%wide.region_6.10_spmd.clone.sunk | while | flops 439489024 | bytes 84838688 | solution.py:121
  79.2 0.8 compare_and_fusion.2
  80.2 5.1 %fusion.152 = (f32[2,512]{1,0:T(2,128)S(1)}, f32[2,512,1024]{1,2,0:T(8,128)S(1)}, f32[2,1024,512]{2,1,0:T(8,128)}) fusion(f32[2,1024]{1,0:T(2,128)S(1)} %dynamic-slice_convert_fusion.3, pred[512,1024]{0,1:T(8,128)(4,1)S(1)} %compare_and_fusion.2, bf16[1024,2,64]{0,2,1:T(8,128)(2,1)S(1)} %bitcast.133, bf16[512,2,64]{0,2,1:T(8,128)(2,1)S(1)} %get-tuple-element.278), kind=kOutput, calls=%fused_computation.33.clone.1 | convolution fusion | flops 145751040 | bytes 9318400 | tf_op jit(solution)/shard_map/while/body/qhd,khd->hqk/dot_general | solution.py:82
  85.2 10.1 %fusion.153 = f32[2,512,8,128]{1,2,3,0:T(8,128)S(1)} fusion(f32[2,512,8,128]{1,3,2,0:T(8,128)S(1)} %bitcast.131), kind=kOutput, calls=%fused_computation.19.clone.1 | output fusion | flops 133169152 | bytes 8388608 | tf_op jit(solution)/shard_map/reduce-window
  95.3 2.0 copy-done
  97.4 2.7 %broadcast_add_fusion.2 = f32[2,512,8,128]{1,2,3,0:T(8,128)S(1)} fusion(f32[2,512,8,128]{1,2,3,0:T(8,128)} %copy-done, f32[2,512,8]{1,2,0:T(8,128)S(1)} %slice.847), kind=kLoop, calls=%fused_computation.22.clone.1 | loop fusion | flops 1048576 | bytes 8421376 | tf_op jit(solution)/shard_map/reduce_window_sum | solution.py:89
  100.1 2.4 %copy.38 = f32[2,512,8,128]{1,3,2,0:T(8,128)S(1)} copy(f32[2,512,8,128]{1,2,3,0:T(8,128)S(1)} %broadcast_add_fusion.2) | data formatting | bytes 8388608 | tf_op jit(solution)/shard_map/reduce_window_sum | solution.py:89
  102.5 6.9 %fusion.154 = bf16[2,512,1024]{1,2,0:T(8,128)(2,1)S(1)} fusion(f32[2,512,8,128]{1,3,2,0:T(8,128)S(1)} %copy.38, f32[2,1024,512]{2,1,0:T(8,128)S(1)} %copy-done.1, f32[2,512]{1,0:T(2,128)S(1)} %get-tuple-element.258, f32[2,1024]{1,0:T(2,128)S(1)} %dynamic-slice_convert_fusion.3, pred[512,1024]{0,1:T(8,128)(4,1)S(1)} %compare_and_fusion.2), kind=kLoop, calls=%fused_computation.7.clone.1 | loop fusion | flops 24117248 | bytes 11022336 | tf_op jit(solution)/shard_map/while/body/convert_element_type | solution.py:90
  110.7 0.7 dynamic-slice_convert_fusion.1
  111.5 3.2 %collective-permute-start = (f32[30,128]{1,0:T(8,128)S(1)}, f32[30,128]{1,0:T(8,128)S(1)}, u32[]{:S(2)}, u32[]{:S(2)}) collective-permute-start(f32[30,128]{1,0:T(8,128)S(1)} %slice.285), channel_id=1, source_target_pairs={{0,8},{8,16},{16,24},{1,9},{9,17},{17,25},{2,10},{10,18},{18,26},{... | collective-permute-start | bytes 46088 | tf_op jit(solution)/shard_map/ppermute | solution.py:13
  114.7 0.8 dynamic_slice.19
  115.9 1.1 fusion.130
  117.0 11.8 %all-reduce = (f32[512]{0:T(512)S(1)}, f32[512]{0:T(512)S(1)}) all-reduce(f32[512]{0:T(512)S(1)} %get-tuple-element.104, f32[512]{0:T(512)S(1)} %get-tuple-element.103), channel_id=1, replica_groups=mesh['sp'=4,'fs'=4,'tp'=2] {'fs','tp'}, use_global_device_ids=true, to_apply=%region_4.0 | all-reduce | flops 1024 | bytes 8192 | tf_op jit(solution)/shard_map/psum | solution.py:63
  128.8 0.9 multiply_convert_fusion
  129.7 35.2 %all-gather.8.cloned.1.call-done = bf16[512,1024]{0,1:T(8,128)(2,1)} async-done(((bf16[512,128]{0,1:T(8,128)(2,1)}), bf16[512,1024]{0,1:T(8,128)(2,1)}) %all-gather.8.cloned.1.call-update) | async-done | bytes 1048592 | tf_op jit(solution)/shard_map/all_gather | solution.py:124
  164.9 1.5 fusion.23
  166.4 2.0 %convolution_multiply_fusion = f32[512,256]{1,0:T(8,128)S(1)} fusion(bf16[512,1024]{0,1:T(8,128)(2,1)} %all-gather.8.cloned.1.call-done, f32[1024]{0:T(1024)S(1)} %copy-done.5, bf16[2048,256]{1,0:T(8,128)(2,1)} %param.27, f32[512]{0:T(512)S(1)} %add_rsqrt_fusion), kind=kOutput, calls=%fused_computation.79 | convolution fusion | flops 270139392 | bytes 2103296 | tf_op jit(solution)/shard_map/dot_general | solution.py:133
  168.5 21.8 %all-gather.6.cloned.1.call-done = bf16[512,1024]{1,0:T(8,128)(2,1)} async-done(((bf16[512,128]{1,0:T(8,128)(2,1)}), bf16[512,1024]{1,0:T(8,128)(2,1)}) %all-gather.6.cloned.1.call-update) | async-done | bytes 1048592 | tf_op jit(solution)/shard_map/all_gather | solution.py:123
  190.3 1.5 fusion.21
  191.8 2.4 %fusion.34 = bf16[512,256]{1,0:T(8,128)(2,1)} fusion(f32[512,256]{1,0:T(8,128)S(1)} %convolution_multiply_fusion, bf16[512,1024]{1,0:T(8,128)(2,1)} %all-gather.6.cloned.1.call-done, f32[1024]{0:T(1024)S(1)} %copy-done.6, bf16[2048,256]{1,0:T(8,128)(2,1)S(1)} %copy-done.3, f32[512]{0:T(512)S(1)} %add_rsqrt_fusion.1), kind=kOutput, calls=%fused_computation.82 | convolution fusion | flops 270401536 | bytes 2365440 | tf_op jit(solution)/shard_map/dot_general | solution.py:132
  (44 shorter events, 2.5 us)
Async XLA Ops:
  6.5 22.2 %copy-start.2 = (bf16[2048,128]{1,0:T(8,128)(2,1)S(1)}, bf16[2048,128]{1,0:T(8,128)(2,1)}, u32[]{:S(2)}) copy-start(bf16[2048,128]{1,0:T(8,128)(2,1)} %param.21) | copy-start | bytes 1572868
  6.5 35.6 %copy-start.4 = (f32[2048]{0:T(1024)S(1)}, f32[2048]{0:T(1024)}, u32[]{:S(2)}) copy-start(f32[2048]{0:T(1024)} %param.16) | copy-start | bytes 24580
  6.5 33.5 %all-gather.4.cloned.1.call-start = ((), (), s32[]{:S(2)}) async-start(), calls=%async_computation | async-start | bytes 2359296 | tf_op jit(solution)/shard_map/all_gather | solution.py:41
  7.3 157.6 %all-gather.8.cloned.1.call-start = ((), (), s32[]{:S(2)}) async-start(), calls=%async_computation.2 | async-start | bytes 1179648 | tf_op jit(solution)/shard_map/all_gather | solution.py:124
  78.7 87.8 %copy-start.5 = (f32[1024]{0:T(1024)S(1)}, f32[1024]{0:T(1024)}, u32[]{:S(2)}) copy-start(f32[1024]{0:T(1024)} %param.26) | copy-start | bytes 12292
  95.3 2.0 copy-start
  100.1 2.4 %copy-start.1 = (f32[2,1024,512]{2,1,0:T(8,128)S(1)}, f32[2,1024,512]{2,1,0:T(8,128)}, u32[]{:S(2)}) copy-start(f32[2,1024,512]{2,1,0:T(8,128)} %get-tuple-element.239) | copy-start | bytes 12582916 | tf_op jit(solution)/shard_map/while
  109.9 81.9 %copy-start.3 = (bf16[2048,256]{1,0:T(8,128)(2,1)S(1)}, bf16[2048,256]{1,0:T(8,128)(2,1)}, u32[]{:S(2)}) copy-start(bf16[2048,256]{1,0:T(8,128)(2,1)} %param.27) | copy-start | bytes 3145732
  109.9 81.9 %copy-start.6 = (f32[1024]{0:T(1024)S(1)}, f32[1024]{0:T(1024)}, u32[]{:S(2)}) copy-start(f32[1024]{0:T(1024)} %param.25) | copy-start | bytes 12292
  110.6 79.7 %all-gather.6.cloned.1.call-start = ((), (), s32[]{:S(2)}) async-start(), calls=%async_computation.1 | async-start | bytes 1179648 | tf_op jit(solution)/shard_map/all_gather | solution.py:123
  111.5 4.4 %collective-permute-start = (f32[30,128]{1,0:T(8,128)S(1)}, f32[30,128]{1,0:T(8,128)S(1)}, u32[]{:S(2)}, u32[]{:S(2)}) collective-permute-start(f32[30,128]{1,0:T(8,128)S(1)} %slice.285), channel_id=1, source_target_pairs={{0,8},{8,16},{16,24},{1,9},{9,17},{17,25},{2,10},{10,18},{18,26},{... | collective-permute-start | bytes 46088 | tf_op jit(solution)/shard_map/ppermute | solution.py:13
Sparse Core Ops, SparseCore 0:
  9.2 30.8 all-gather.3
  110.7 54.1 all-gather.7
  166.8 23.4 all-gather.5
where the time goes:
time: 201 us
  waiting for transfers between devices  68.6 us (34%)
  blocking collectives  57.7 us (29%)
  other arithmetic  29.1 us (14%)
  local copies, waits for them, and re-layouts  14.3 us (7%)
  matrix products  14.1 us (7%)
  between operations  13.3 us (7%)
  starting transfers between devices  3.27 us (2%)
    all_gather x1, waiting for transfers between devices, per_device(): attn_piece = lax.all_gather(attn_mixed, ('fs', 'tp'), axis=1, tiled=True)  35.2 us
    all_gather x1, waiting for transfers between devices, per_device(): conv_piece = lax.all_gather(conv_mixed, ('fs', 'tp'), axis=1, tiled=True)  21.8 us
    all_gather x1, blocking collectives, per_device(): lax.all_gather(value, 'sp', axis=0, tiled=True)  16.1 us
    all_gather x1, blocking collectives, per_device(): lax.all_gather(key, 'sp', axis=0, tiled=True)  16 us
    all_gather x1, blocking collectives, per_device(): lax.all_gather(break_shift, 'sp', axis=1, tiled=True)  13.8 us
    psum x1, blocking collectives, per_device(): lax.psum((jnp.sum(conv_out, axis=1), jnp.sum(conv_out * conv_out, axis=1)...  11.8 us
    all_gather x1, waiting for transfers between devices, per_device(): segment = lax.all_gather(tokens, ('fs', 'tp'), axis=1, tiled=True)  10.4 us
    another operation x2, other arithmetic  10.1 us
  transfers between devices with their start and end apart: 4, of which 4 were waited for; matrix products, arithmetic and copies ran while one was open for 8% of the time, Pallas kernels for 0%

commit v1 on v0

--- a/solution.py
+++ b/solution.py
@@ -102,7 +102,7 @@
     all_keys, all_values, all_shifts = (
         lax.all_gather(key, "sp", axis=0, tiled=True),
         lax.all_gather(value, "sp", axis=0, tiled=True),
-        lax.all_gather(break_shift, "sp", axis=1, tiled=True),
+        jnp.concatenate(lax.all_gather(break_shift, "sp"), axis=1),
     )
     sp_count = lax.axis_size("sp")
     grouped = 1

time: 201 us -> 201 us (level)
  no operation moved by 1% of the time
where the time goes in v1:
time: 201 us
  waiting for transfers between devices  68.6 us (34%)
  blocking collectives  57.7 us (29%)
  other arithmetic  29.1 us (14%)
  local copies, waits for them, and re-layouts  14.3 us (7%)
  matrix products  14.1 us (7%)
  between operations  13.3 us (7%)
  starting transfers between devices  3.27 us (2%)
    all_gather x1, waiting for transfers between devices, per_device(): attn_piece = lax.all_gather(attn_mixed, ('fs', 'tp'), axis=1, tiled=True)  35.2 us
    all_gather x1, waiting for transfers between devices, per_device(): conv_piece = lax.all_gather(conv_mixed, ('fs', 'tp'), axis=1, tiled=True)  21.8 us
    all_gather x1, blocking collectives, per_device(): lax.all_gather(value, 'sp', axis=0, tiled=True)  16.1 us
    all_gather x1, blocking collectives, per_device(): lax.all_gather(key, 'sp', axis=0, tiled=True)  16 us
    all_gather x1, blocking collectives, per_device(): lax.all_gather(break_shift, 'sp')  13.8 us
    psum x1, blocking collectives, per_device(): lax.psum((jnp.sum(conv_out, axis=1), jnp.sum(conv_out * conv_out, axis=1)...  11.8 us
    all_gather x1, waiting for transfers between devices, per_device(): segment = lax.all_gather(tokens, ('fs', 'tp'), axis=1, tiled=True)  10.4 us
    another operation x2, other arithmetic  10.1 us
  transfers between devices with their start and end apart: 4, of which 4 were waited for; matrix products, arithmetic and copies ran while one was open for 8% of the time, Pallas kernels for 0%

profile of v1, /device:TPU:0, one launch (start us, length us, event | category | flops | bytes accessed | tf_op | source)
XLA Modules:
  0.0 200.8 jit_solution(3201915320007578196)
XLA Ops:
  6.5 0.7 all-gather.6.cloned.1.call-update
  7.3 13.8 %all-gather.1 = bf16[4,2,512]{2,1,0:T(2,128)(2,1)S(1)} all-gather(bf16[1,2,512]{2,1,0:T(2,128)(2,1)} %bitcast.141), channel_id=2, replica_groups=mesh['sp'=4,'fs'=4,'tp'=2] {'sp'}, dimensions={0}, use_global_device_ids=true | all-gather | bytes 10240 | tf_op jit(solution)/shard_map/all_gather | solution.py:105
  21.1 1.9 constant_dynamic-update-slice_fusion.4
  23.0 1.9 constant_dynamic-update-slice_fusion.3
  24.9 1.9 constant_dynamic-update-slice_fusion.2
  26.9 1.9 constant_dynamic-update-slice_fusion.1
  28.8 0.9 constant_dynamic-update-slice_fusion
  29.6 10.4 %all-gather.6.cloned.1.call-done = bf16[512,2048]{1,0:T(8,128)(2,1)} async-done(((bf16[512,256]{1,0:T(8,128)(2,1)}), bf16[512,2048]{1,0:T(8,128)(2,1)}) %all-gather.6.cloned.1.call-update) | async-done | bytes 2097168 | tf_op jit(solution)/shard_map/all_gather | solution.py:41
  40.1 2.1 %fusion.19 = f32[512]{0:T(512)S(1)} fusion(bf16[512,2048]{1,0:T(8,128)(2,1)} %all-gather.6.cloned.1.call-done), kind=kLoop, calls=%fused_computation.37 | loop fusion | flops 3145216 | bytes 2099200 | tf_op jit(solution)/shard_map/reduce_sum | solution.py:45
  42.2 4.2 %fusion.30 = bf16[512,640]{1,0:T(8,128)(2,1)S(1)} fusion(bf16[2048,640]{1,0:T(8,128)(2,1)} %constant_dynamic-update-slice_fusion, bf16[512,2048]{1,0:T(8,128)(2,1)} %all-gather.6.cloned.1.call-done, f32[2048]{0:T(1024)S(1)} %copy-done.4, f32[512]{0:T(512)S(1)} %add_rsqrt_fusion.3), kind=kOutput, calls=%fused_computation.78 | convolution fusion | flops 1345978368 | bytes 5384192 | tf_op jit(solution)/shard_map/dot_general | solution.py:44
  46.4 16.1 %all_gather.23 = bf16[2048,128]{1,0:T(8,128)(2,1)S(1)} all-gather(bf16[512,128]{1,0:T(8,128)(2,1)S(1)} %get-tuple-element.145), channel_id=1, replica_groups=mesh['sp'=4,'fs'=4,'tp'=2] {'sp'}, dimensions={0}, use_global_device_ids=true | all-gather | bytes 655360 | tf_op jit(solution)/shard_map/all_gather | solution.py:104
  62.5 16.0 %all_gather.24 = bf16[2048,128]{1,0:T(8,128)(2,1)S(1)} all-gather(bf16[512,128]{1,0:T(8,128)(2,1)S(1)} %get-tuple-element.144), channel_id=1, replica_groups=mesh['sp'=4,'fs'=4,'tp'=2] {'sp'}, dimensions={0}, use_global_device_ids=true | all-gather | bytes 655360 | tf_op jit(solution)/shard_map/all_gather | solution.py:103
  78.7 31.2 %while.13 = (s32[]{:T(128)}, f32[512,2,64]{0,2,1:T(8,128)S(1)}, f32[2,512]{1,0:T(2,128)S(1)}, s32[]{:T(128)}, s32[]{:T(128)}, /*index=5*/bf16[2048,128]{1,0:T(8,...) while((s32[]{:T(128)}, f32[512,2,64]{0,2,1:T(8,128)S(1)}, ...), condition=%wide.region_10.11_spmd.clone, body=%wide.region_6.10_spmd.clone.sunk | while | flops 439489024 | bytes 84838688 | solution.py:121
  79.2 0.8 compare_and_fusion.2
  80.2 5.1 %fusion.152 = (f32[2,512]{1,0:T(2,128)S(1)}, f32[2,512,1024]{1,2,0:T(8,128)S(1)}, f32[2,1024,512]{2,1,0:T(8,128)}) fusion(f32[2,1024]{1,0:T(2,128)S(1)} %dynamic-slice_convert_fusion.3, pred[512,1024]{0,1:T(8,128)(4,1)S(1)} %compare_and_fusion.2, bf16[1024,2,64]{0,2,1:T(8,128)(2,1)S(1)} %bitcast.137, bf16[512,2,64]{0,2,1:T(8,128)(2,1)S(1)} %get-tuple-element.288), kind=kOutput, calls=%fused_computation.33.clone.1 | convolution fusion | flops 145751040 | bytes 9318400 | tf_op jit(solution)/shard_map/while/body/qhd,khd->hqk/dot_general | solution.py:82
  85.2 10.1 %fusion.153 = f32[2,512,8,128]{1,2,3,0:T(8,128)S(1)} fusion(f32[2,512,8,128]{1,3,2,0:T(8,128)S(1)} %bitcast.135), kind=kOutput, calls=%fused_computation.19.clone.1 | output fusion | flops 133169152 | bytes 8388608 | tf_op jit(solution)/shard_map/reduce-window
  95.3 2.0 copy-done
  97.4 2.7 %broadcast_add_fusion.2 = f32[2,512,8,128]{1,2,3,0:T(8,128)S(1)} fusion(f32[2,512,8,128]{1,2,3,0:T(8,128)} %copy-done, f32[2,512,8]{1,2,0:T(8,128)S(1)} %slice.847), kind=kLoop, calls=%fused_computation.22.clone.1 | loop fusion | flops 1048576 | bytes 8421376 | tf_op jit(solution)/shard_map/reduce_window_sum | solution.py:89
  100.1 2.4 %copy.44 = f32[2,512,8,128]{1,3,2,0:T(8,128)S(1)} copy(f32[2,512,8,128]{1,2,3,0:T(8,128)S(1)} %broadcast_add_fusion.2) | data formatting | bytes 8388608 | tf_op jit(solution)/shard_map/reduce_window_sum | solution.py:89
  102.5 6.9 %fusion.154 = bf16[2,512,1024]{1,2,0:T(8,128)(2,1)S(1)} fusion(f32[2,512,8,128]{1,3,2,0:T(8,128)S(1)} %copy.44, f32[2,1024,512]{2,1,0:T(8,128)S(1)} %copy-done.1, f32[2,512]{1,0:T(2,128)S(1)} %get-tuple-element.268, f32[2,1024]{1,0:T(2,128)S(1)} %dynamic-slice_convert_fusion.3, pred[512,1024]{0,1:T(8,128)(4,1)S(1)} %compare_and_fusion.2), kind=kLoop, calls=%fused_computation.7.clone.1 | loop fusion | flops 24117248 | bytes 11022336 | tf_op jit(solution)/shard_map/while/body/convert_element_type | solution.py:90
  110.7 0.7 dynamic-slice_convert_fusion.1
  111.5 3.2 %collective-permute-start = (f32[30,128]{1,0:T(8,128)S(1)}, f32[30,128]{1,0:T(8,128)S(1)}, u32[]{:S(2)}, u32[]{:S(2)}) collective-permute-start(f32[30,128]{1,0:T(8,128)S(1)} %slice.285), channel_id=1, source_target_pairs={{0,8},{8,16},{16,24},{1,9},{9,17},{17,25},{2,10},{10,18},{18,26},{... | collective-permute-start | bytes 46088 | tf_op jit(solution)/shard_map/ppermute | solution.py:13
  114.7 0.8 dynamic_slice.19
  115.9 1.1 fusion.130
  117.0 11.8 %all-reduce = (f32[512]{0:T(512)S(1)}, f32[512]{0:T(512)S(1)}) all-reduce(f32[512]{0:T(512)S(1)} %get-tuple-element.114, f32[512]{0:T(512)S(1)} %get-tuple-element.113), channel_id=1, replica_groups=mesh['sp'=4,'fs'=4,'tp'=2] {'fs','tp'}, use_global_device_ids=true, to_apply=%region_4.0 | all-reduce | flops 1024 | bytes 8192 | tf_op jit(solution)/shard_map/psum | solution.py:63
  128.8 0.9 multiply_convert_fusion
  129.7 35.2 %all-gather.10.cloned.1.call-done = bf16[512,1024]{0,1:T(8,128)(2,1)} async-done(((bf16[512,128]{0,1:T(8,128)(2,1)}), bf16[512,1024]{0,1:T(8,128)(2,1)}) %all-gather.10.cloned.1.call-update) | async-done | bytes 1048592 | tf_op jit(solution)/shard_map/all_gather | solution.py:124
  164.9 1.5 fusion.23
  166.4 2.0 %convolution_multiply_fusion = f32[512,256]{1,0:T(8,128)S(1)} fusion(bf16[512,1024]{0,1:T(8,128)(2,1)} %all-gather.10.cloned.1.call-done, f32[1024]{0:T(1024)S(1)} %copy-done.5, bf16[2048,256]{1,0:T(8,128)(2,1)} %param.27, f32[512]{0:T(512)S(1)} %add_rsqrt_fusion), kind=kOutput, calls=%fused_computation.79 | convolution fusion | flops 270139392 | bytes 2103296 | tf_op jit(solution)/shard_map/dot_general | solution.py:133
  168.5 21.8 %all-gather.8.cloned.1.call-done = bf16[512,1024]{1,0:T(8,128)(2,1)} async-done(((bf16[512,128]{1,0:T(8,128)(2,1)}), bf16[512,1024]{1,0:T(8,128)(2,1)}) %all-gather.8.cloned.1.call-update) | async-done | bytes 1048592 | tf_op jit(solution)/shard_map/all_gather | solution.py:123
  190.3 1.5 fusion.21
  191.8 2.4 %fusion.34 = bf16[512,256]{1,0:T(8,128)(2,1)} fusion(f32[512,256]{1,0:T(8,128)S(1)} %convolution_multiply_fusion, bf16[512,1024]{1,0:T(8,128)(2,1)} %all-gather.8.cloned.1.call-done, f32[1024]{0:T(1024)S(1)} %copy-done.6, bf16[2048,256]{1,0:T(8,128)(2,1)S(1)} %copy-done.3, f32[512]{0:T(512)S(1)} %add_rsqrt_fusion.1), kind=kOutput, calls=%fused_computation.82 | convolution fusion | flops 270401536 | bytes 2365440 | tf_op jit(solution)/shard_map/dot_general | solution.py:132
  (44 shorter events, 2.5 us)
Async XLA Ops:
  6.5 22.2 %copy-start.2 = (bf16[2048,128]{1,0:T(8,128)(2,1)S(1)}, bf16[2048,128]{1,0:T(8,128)(2,1)}, u32[]{:S(2)}) copy-start(bf16[2048,128]{1,0:T(8,128)(2,1)} %param.21) | copy-start | bytes 1572868
  6.5 35.6 %copy-start.4 = (f32[2048]{0:T(1024)S(1)}, f32[2048]{0:T(1024)}, u32[]{:S(2)}) copy-start(f32[2048]{0:T(1024)} %param.16) | copy-start | bytes 24580
  6.5 33.5 %all-gather.6.cloned.1.call-start = ((), (), s32[]{:S(2)}) async-start(), calls=%async_computation | async-start | bytes 2359296 | tf_op jit(solution)/shard_map/all_gather | solution.py:41
  7.3 157.6 %all-gather.10.cloned.1.call-start = ((), (), s32[]{:S(2)}) async-start(), calls=%async_computation.2 | async-start | bytes 1179648 | tf_op jit(solution)/shard_map/all_gather | solution.py:124
  78.7 87.8 %copy-start.5 = (f32[1024]{0:T(1024)S(1)}, f32[1024]{0:T(1024)}, u32[]{:S(2)}) copy-start(f32[1024]{0:T(1024)} %param.26) | copy-start | bytes 12292
  95.3 2.0 copy-start
  100.1 2.4 %copy-start.1 = (f32[2,1024,512]{2,1,0:T(8,128)S(1)}, f32[2,1024,512]{2,1,0:T(8,128)}, u32[]{:S(2)}) copy-start(f32[2,1024,512]{2,1,0:T(8,128)} %get-tuple-element.249) | copy-start | bytes 12582916 | tf_op jit(solution)/shard_map/while
  109.9 81.9 %copy-start.3 = (bf16[2048,256]{1,0:T(8,128)(2,1)S(1)}, bf16[2048,256]{1,0:T(8,128)(2,1)}, u32[]{:S(2)}) copy-start(bf16[2048,256]{1,0:T(8,128)(2,1)} %param.27) | copy-start | bytes 3145732
  109.9 81.9 %copy-start.6 = (f32[1024]{0:T(1024)S(1)}, f32[1024]{0:T(1024)}, u32[]{:S(2)}) copy-start(f32[1024]{0:T(1024)} %param.25) | copy-start | bytes 12292
  110.6 79.7 %all-gather.8.cloned.1.call-start = ((), (), s32[]{:S(2)}) async-start(), calls=%async_computation.1 | async-start | bytes 1179648 | tf_op jit(solution)/shard_map/all_gather | solution.py:123
  111.5 4.4 %collective-permute-start = (f32[30,128]{1,0:T(8,128)S(1)}, f32[30,128]{1,0:T(8,128)S(1)}, u32[]{:S(2)}, u32[]{:S(2)}) collective-permute-start(f32[30,128]{1,0:T(8,128)S(1)} %slice.285), channel_id=1, source_target_pairs={{0,8},{8,16},{16,24},{1,9},{9,17},{17,25},{2,10},{10,18},{18,26},{... | collective-permute-start | bytes 46088 | tf_op jit(solution)/shard_map/ppermute | solution.py:13
Sparse Core Ops, SparseCore 0:
  9.2 30.8 all-gather.5
  110.7 54.1 all-gather.9
  166.8 23.4 all-gather.7
